TPU v7x, 32 devices: a whole 2x2x4 slice. The times are simulated.
32 devices in a mesh: sp: 16 (over z, y, x), tp: 2 (over core).
Axes of the slice: x: 2, y: 2, z: 4, core: 2. Of those that a mesh axis runs over, the one named last changes fastest.
Arguments:
- resid: bfloat16 [3072, 2048], P('sp'), may hold values from -6 to 6
- query: bfloat16 [3072, 2048], P('sp', 'tp'), may hold values from -6 to 6
- key: bfloat16 [3072, 1024], P('sp', 'tp'), may hold values from -6 to 6
- value: bfloat16 [3072, 1024], P('sp', 'tp'), may hold values from -6 to 6
- q_gain: float32 [128], replicated, may hold values from 0.3 to 5, as said below
- k_gain: float32 [128], replicated, may hold values from 0.3 to 5, as said below
- out_weight: bfloat16 [2048, 2048], P('tp'), may hold values from -0.125 to 0.125
- norm_gain: float32 [2048], replicated, may hold values from 0.1 to 1.9
- gate_weight: bfloat16 [2048, 5632], P('sp', 'tp'), may hold values from -0.125 to 0.125
- up_weight: bfloat16 [2048, 5632], P('sp', 'tp'), may hold values from -0.125 to 0.125
- down_weight: bfloat16 [5632, 2048], P('tp', 'sp'), may hold values from -0.078125 to 0.078125
Outputs:
- mixed: bfloat16 [3072, 2048], P(('sp', 'tp'))
Inputs may be any that keep to these rules, and one draw needn't show every extreme that they name: `q_gain`: positive gains. `k_gain`: positive gains.
All inputs are finite; a program needn't handle non-finite values.
Results may differ from a plain program's by a relative error of at most 0.012.
The roundings to bfloat16 on the way count: a program that leaves them out, or rounds other values in their place, can miss the bound.
Values may be sent and summed in bfloat16 or wider, within the bound.
A program may use at most 128 MiB of HBM per device.

v0:
```python
import jax
import jax.numpy as jnp
from jax import lax
from jax.sharding import PartitionSpec as P

GRID_W = 64
EPSILON = 1e-06


def rotate(values, positions):
    dim_size = values.shape[-1]
    half_dim = dim_size // 2
    quarter = half_dim // 2
    inverse = 10000.0 ** (-jnp.arange(quarter, dtype=jnp.float32) / quarter)
    outputs = []
    for axis_pos, coords in enumerate((positions // GRID_W, positions % GRID_W)):
        angles = coords.astype(jnp.float32)[:, None] * inverse[None, :]
        cosine = jnp.cos(angles)[:, None, :]
        sine = jnp.sin(angles)[:, None, :]
        section = values[..., axis_pos * half_dim : (axis_pos + 1) * half_dim]
        first_half = section[..., :quarter]
        second_half = section[..., quarter:]
        outputs += [
            first_half * cosine - second_half * sine,
            second_half * cosine + first_half * sine,
        ]
    return jnp.concatenate(outputs, axis=-1)


def prepare(projected, gain, positions):
    values = projected.astype(jnp.float32)
    normed = values * lax.rsqrt(jnp.mean(values * values, axis=-1, keepdims=True) + EPSILON) * gain
    return rotate(normed, positions).astype(jnp.bfloat16)


def normalize(stream, gain):
    values = stream.astype(jnp.float32)
    return (
        values * lax.rsqrt(jnp.mean(values * values, axis=-1, keepdims=True) + EPSILON) * gain
    ).astype(jnp.bfloat16)


def body(
    resid,
    query,
    key,
    value,
    q_gain,
    k_gain,
    out_weight,
    norm_gain,
    gate_weight,
    up_weight,
    down_weight,
):
    rows_here = query.shape[0]
    head_dim = q_gain.shape[0]
    heads_here = query.shape[1] // head_dim
    kv_here = key.shape[1] // head_dim
    group_size = heads_here // kv_here
    score_scale = head_dim ** (-0.5)
    positions = lax.axis_index("sp") * rows_here + jnp.arange(rows_here, dtype=jnp.int32)
    q_rot = prepare(query.reshape(rows_here, heads_here, head_dim), q_gain, positions)
    k_rot = prepare(key.reshape(rows_here, kv_here, head_dim), k_gain, positions)
    val_rows = value.reshape(rows_here, kv_here, head_dim)
    grouped = q_rot.reshape(rows_here, kv_here, group_size, head_dim)

    def key_block(carry, block):
        maxima, totals, accum = carry
        block_keys, block_vals = block
        scores = (
            jnp.einsum("qkgd,skd->kgqs", grouped, block_keys, preferred_element_type=jnp.float32)
            * score_scale
        )
        new_max = jnp.maximum(maxima, jnp.max(scores, axis=-1))
        shrink = jnp.exp(maxima - new_max)
        weights = jnp.exp(scores - new_max[..., None])
        totals = totals * shrink + jnp.sum(weights, axis=-1)
        accum = accum * shrink[..., None] + jnp.einsum(
            "kgqs,skd->kgqd",
            weights.astype(jnp.bfloat16),
            block_vals,
            preferred_element_type=jnp.float32,
        )
        return ((new_max, totals, accum), None)

    start_max = jnp.full((kv_here, group_size, rows_here), -1e30, jnp.float32)
    start_total = jnp.zeros((kv_here, group_size, rows_here), jnp.float32)
    start_accum = jnp.zeros((kv_here, group_size, rows_here, head_dim), jnp.float32)
    carry = (start_max, start_total, start_accum)
    key_part = lax.all_gather(k_rot, "sp", axis=0, tiled=True)
    val_part = lax.all_gather(val_rows, "sp", axis=0, tiled=True)
    length = key_part.shape[0]
    factor = 4
    span = rows_here * factor
    turns = length // span
    key_blocks = key_part.reshape(turns, span, kv_here, head_dim)
    val_blocks = val_part.reshape(turns, span, kv_here, head_dim)
    carry, _ = lax.scan(key_block, carry, (key_blocks, val_blocks))
    maxima, totals, accum = carry
    attn = (
        jnp.transpose(accum / totals[..., None], (2, 0, 1, 3))
        .reshape(rows_here, heads_here * head_dim)
        .astype(jnp.bfloat16)
    )
    share = rows_here // lax.axis_size("tp")
    my_first = lax.axis_index("tp") * share
    proj = lax.psum_scatter(
        jnp.dot(attn, out_weight, preferred_element_type=jnp.float32).astype(jnp.bfloat16),
        "tp",
        scatter_dimension=0,
        tiled=True,
    ).astype(jnp.float32)
    my_resid = lax.dynamic_slice_in_dim(resid, my_first, share, 0)
    my_stream = (my_resid.astype(jnp.float32) + proj).astype(jnp.bfloat16)
    mixer_rows = lax.all_gather(normalize(my_stream, norm_gain), "tp", axis=0, tiled=True)

    def add_rows(shard_rows):
        return jnp.dot(mixer_rows, shard_rows, preferred_element_type=jnp.float32)

    gate = add_rows(lax.all_gather(gate_weight, "sp", axis=0, tiled=True))
    up_part = add_rows(lax.all_gather(up_weight, "sp", axis=0, tiled=True))
    hidden = (jax.nn.silu(gate) * up_part).astype(jnp.bfloat16)
    down_whole = lax.all_gather(down_weight, "sp", axis=1, tiled=True)
    down = lax.psum_scatter(
        jnp.dot(hidden, down_whole, preferred_element_type=jnp.float32).astype(jnp.bfloat16),
        "tp",
        scatter_dimension=0,
        tiled=True,
    ).astype(jnp.float32)
    return (my_stream.astype(jnp.float32) + 0.5 * down).astype(jnp.bfloat16)


def solution(mesh):
    placed = (
        P("sp", None),
        P("sp", "tp"),
        P("sp", "tp"),
        P("sp", "tp"),
        P(),
        P(),
        P("tp", None),
        P(),
        P("sp", "tp"),
        P("sp", "tp"),
        P("tp", "sp"),
    )
    return jax.shard_map(
        body, mesh=mesh, in_specs=placed, out_specs=P(("sp", "tp"), None), check_vma=False
    )
```

profile of v0, /device:TPU:0, one launch (start us, length us, event | category | flops | bytes accessed | tf_op | source)
XLA Modules:
  0.0 702.4 jit_solution(25329568361684075)
XLA Ops:
  6.6 1.1 reshape.193
  10.4 1.3 pad_maximum_fusion.1
  15.1 67.4 %all-gather.6.cloned.1.call-done = bf16[3072,4,128]{2,1,0:T(4,128)(2,1)} async-done(((bf16[192,4,128]{2,1,0:T(4,128)(2,1)}), bf16[3072,4,128]{2,1,0:T(4,128)(2,1)}) %all-gather.6.cloned.1.call-update) | async-done | bytes 3145744 | tf_op jit(solution)/shard_map/all_gather | solution.py:91
  82.5 69.2 %all-gather.8.cloned.1.call-done = bf16[3072,4,128]{2,1,0:T(4,128)(2,1)} async-done(((bf16[192,4,128]{2,1,0:T(4,128)(2,1)}), bf16[3072,4,128]{2,1,0:T(4,128)(2,1)}) %all-gather.8.cloned.1.call-update) | async-done | bytes 3145744 | tf_op jit(solution)/shard_map/all_gather | solution.py:92
  151.7 40.1 %while.15 = (s32[]{:T(128)}, f32[4,2,192]{2,1,0:T(2,128)S(1)}, f32[4,2,192]{2,1,0:T(2,128)S(1)}, f32[4,2,192,128]{3,2,1,0:T(8,128)S(1)}, bf16[4,768,4,128]{3,2,1...) while((s32[]{:T(128)}, f32[4,2,192]{2,1,0:T(2,128)S(1)}, ...), condition=%wide.region_5.6_spmd.clone, body=%wide.region_2.5_spmd.clone.sunk | while | flops 614014464 | bytes 39813256 | solution.py:99
  151.7 1.9 constant_dynamic-slice_fusion.3
  153.6 2.9 bitcast_reduce_fusion.2
  156.5 3.5 fusion.42
  160.3 1.4 fusion.44
  161.7 1.9 constant_dynamic-slice_fusion.3
  163.6 2.9 bitcast_reduce_fusion.2
  166.6 3.5 fusion.42
  170.3 1.4 fusion.44
  171.7 1.9 constant_dynamic-slice_fusion.3
  173.6 2.9 bitcast_reduce_fusion.2
  176.6 3.5 fusion.42
  180.3 1.4 fusion.44
  181.7 1.9 constant_dynamic-slice_fusion.3
  183.7 2.9 bitcast_reduce_fusion.2
  186.6 3.5 fusion.42
  190.3 1.4 fusion.44
  192.8 4.1 convolution_convert_fusion.1
  198.7 5.1 reduce-scatter.3.cloned.1.call-done
  203.8 1.2 fusion.15
  205.2 2.5 all_gather.20
  207.7 141.2 %all-gather.10.cloned.1.call-done = bf16[2048,2816]{1,0:T(8,128)(2,1)} async-done(((bf16[128,2816]{1,0:T(8,128)(2,1)}), bf16[2048,2816]{1,0:T(8,128)(2,1)}) %all-gather.10.cloned.1.call-update) | async-done | bytes 11534352 | tf_op jit(solution)/shard_map/all_gather | solution.py:121
  348.9 6.7 fusion.24
  355.6 135.6 %all-gather.12.cloned.1.call-done = bf16[2048,2816]{1,0:T(8,128)(2,1)} async-done(((bf16[128,2816]{1,0:T(8,128)(2,1)}), bf16[2048,2816]{1,0:T(8,128)(2,1)}) %all-gather.12.cloned.1.call-update) | async-done | bytes 11534352 | tf_op jit(solution)/shard_map/all_gather | solution.py:122
  491.2 182.8 %all-gather.14.cloned.1.call-done = bf16[2816,2048]{1,0:T(8,128)(2,1)} async-done(((bf16[2816,128]{1,0:T(8,128)(2,1)}), bf16[2816,2048]{1,0:T(8,128)(2,1)}) %all-gather.14.cloned.1.call-update) | async-done | bytes 11534352 | tf_op jit(solution)/shard_map/all_gather | solution.py:124
  674.0 13.2 %convolution_convert_fusion = bf16[192,2048]{1,0:T(8,128)(2,1)} fusion(bf16[2816,2048]{1,0:T(8,128)(2,1)} %all-gather.14.cloned.1.call-done, bf16[192,2048]{1,0:T(8,128)(2,1)S(1)} %all_gather.20, bf16[2048,2816]{1,0:T(8,128)(2,1)} %all-gather.12.cloned.1.call-done, f32[192,2816]{1,0:T(8,128)S(1)} %fusion.24), kind=kOutput, calls=%fused_computation.23 | convolution fusion | flops 4432822272 | bytes 26804224 | tf_op jit(solution)/shard_map/dot_general | solution.py:126
  687.2 6.5 reduce-scatter.5.cloned.1.call-done
  693.7 1.9 fusion.18
  (73 shorter events, 9.7 us)
Async XLA Ops:
  6.5 5.2 copy-start.2
  6.5 6.1 copy-start.1
  6.5 75.9 %all-gather.6.cloned.1.call-start = ((), (), s32[]{:S(2)}) async-start(), calls=%async_computation.2 | async-start | bytes 3342336 | tf_op jit(solution)/shard_map/all_gather | solution.py:91
  8.0 5.3 copy-start.5
  11.7 140.0 %all-gather.8.cloned.1.call-start = ((), (), s32[]{:S(2)}) async-start(), calls=%async_computation.3 | async-start | bytes 3342336 | tf_op jit(solution)/shard_map/all_gather | solution.py:92
  12.5 191.2 %reduce-scatter.3.cloned.1.call-start = ((), (), s32[]{:S(2)}) async-start(), calls=%async_computation.4 | async-start | bytes 1179648 | tf_op jit(solution)/shard_map/reduce_scatter | solution.py:108
  156.5 3.8 copy-start
  166.5 3.8 copy-start
  176.6 3.8 copy-start
  186.6 3.8 copy-start
  192.5 11.3 %copy-start.3 = (bf16[192,2048]{1,0:T(8,128)(2,1)S(1)}, bf16[192,2048]{1,0:T(8,128)(2,1)}, u32[]{:S(2)}) copy-start(bf16[192,2048]{1,0:T(8,128)(2,1)} %param.13) | copy-start | bytes 2359300
  192.7 12.3 %copy-start.4 = (f32[2048]{0:T(1024)S(1)}, f32[2048]{0:T(1024)}, u32[]{:S(2)}) copy-start(f32[2048]{0:T(1024)} %param.20) | copy-start | bytes 24580
  196.9 152.0 %all-gather.10.cloned.1.call-start = ((), (), s32[]{:S(2)}) async-start(), calls=%async_computation.5 | async-start | bytes 12255232 | tf_op jit(solution)/shard_map/all_gather | solution.py:121
  197.5 293.7 %all-gather.12.cloned.1.call-start = ((), (), s32[]{:S(2)}) async-start(), calls=%async_computation.6 | async-start | bytes 12255232 | tf_op jit(solution)/shard_map/all_gather | solution.py:122
  198.1 475.9 %all-gather.14.cloned.1.call-start = ((), (), s32[]{:S(2)}) async-start(), calls=%async_computation.7 | async-start | bytes 12255232 | tf_op jit(solution)/shard_map/all_gather | solution.py:124
  198.6 495.1 %reduce-scatter.5.cloned.1.call-start = ((), (), s32[]{:S(2)}) async-start(), calls=%async_computation.8 | async-start | bytes 1179648 | tf_op jit(solution)/shard_map/reduce_scatter | solution.py:125
Sparse Core Ops, SparseCore 0:
  11.9 70.5 all-gather.5
  85.2 66.3 all-gather.7
  197.0 6.6 reduce-scatter.2
  206.4 142.5 all-gather.9
  351.5 139.5 all-gather.11
  493.7 180.2 all-gather.13
  687.3 6.3 reduce-scatter.4
where the time goes:
time: 703 us; the launch traced here: 702 us
  waiting for transfers between devices  609 us (87%)
  matrix products  41.2 us (6%)
  other arithmetic  23.7 us (3%)
  between operations  13.8 us (2%)
  local copies, waits for them, and re-layouts  11.4 us (2%)
    all_gather x1, waiting for transfers between devices, body(): down_whole = lax.all_gather(down_weight, 'sp', axis=1, tiled=True)  183 us
    all_gather x1, waiting for transfers between devices, body(): gate = add_rows(lax.all_gather(gate_weight, 'sp', axis=0, tiled=True))  141 us
    all_gather x1, waiting for transfers between devices, body(): up_part = add_rows(lax.all_gather(up_weight, 'sp', axis=0, tiled=True))  136 us
    all_gather x1, waiting for transfers between devices, body(): val_part = lax.all_gather(val_rows, 'sp', axis=0, tiled=True)  69.2 us
    all_gather x1, waiting for transfers between devices, body(): key_part = lax.all_gather(k_rot, 'sp', axis=0, tiled=True)  67.4 us
    reduce_sum x4, other arithmetic, key_block(): totals = totals * shrink + jnp.sum(weights, axis=-1)  14.2 us
  transfers between devices with their start and end apart: 7, of which 7 were waited for; matrix products, arithmetic and copies ran while one was open for 2% of the time, Pallas kernels for 0%

commit v1 on v0

--- a/solution.py
+++ b/solution.py
@@ -121,7 +121,7 @@
     gate = add_rows(lax.all_gather(gate_weight, "sp", axis=0, tiled=True))
     up_part = add_rows(lax.all_gather(up_weight, "sp", axis=0, tiled=True))
     hidden = (jax.nn.silu(gate) * up_part).astype(jnp.bfloat16)
-    down_whole = lax.all_gather(down_weight, "sp", axis=1, tiled=True)
+    down_whole = jnp.concatenate(lax.all_gather(down_weight, "sp"), axis=1)
     down = lax.psum_scatter(
         jnp.dot(hidden, down_whole, preferred_element_type=jnp.float32).astype(jnp.bfloat16),
         "tp",

time: 703 us -> 664 us (0.945)
  waiting for transfers between devices: 609 us -> 554 us
  local copies, waits for them, and re-layouts: 11.4 us -> 26.6 us
    all_gather x1, waiting for transfers between devices: 183 us -> 141 us  [body(): down_whole = jnp.concatenate(lax.all_gather(down_weight, 'sp'), axis=1)]
    reshape x0 -> x1, local copies, waits for them, and re-layouts: none -> 15.1 us  [body(): down_whole = jnp.concatenate(lax.all_gather(down_weight, 'sp'), axis=1)]
    all_gather x1, waiting for transfers between devices: 141 us -> 127 us  [body(): gate = add_rows(lax.all_gather(gate_weight, 'sp', axis=0, tiled=True))]
  transfers between devices with their start and end apart: 7 -> 7, of which waited for: 7 -> 7; matrix products, arithmetic and copies ran while one was open for 2% -> 4% of each run, Pallas kernels for 0% -> 0%
where the time goes in v1:
time: 664 us; the launch traced here: 663 us
  waiting for transfers between devices  554 us (83%)
  matrix products  42.6 us (6%)
  local copies, waits for them, and re-layouts  26.6 us (4%)
  other arithmetic  23.7 us (4%)
  between operations  13.8 us (2%)
    all_gather x1, waiting for transfers between devices, body(): down_whole = jnp.concatenate(lax.all_gather(down_weight, 'sp'), axis=1)  141 us
    all_gather x1, waiting for transfers between devices, body(): up_part = add_rows(lax.all_gather(up_weight, 'sp', axis=0, tiled=True))  136 us
    all_gather x1, waiting for transfers between devices, body(): gate = add_rows(lax.all_gather(gate_weight, 'sp', axis=0, tiled=True))  127 us
    all_gather x1, waiting for transfers between devices, body(): val_part = lax.all_gather(val_rows, 'sp', axis=0, tiled=True)  69.2 us
    all_gather x1, waiting for transfers between devices, body(): key_part = lax.all_gather(k_rot, 'sp', axis=0, tiled=True)  67.4 us
    reshape x1, local copies, waits for them, and re-layouts, body(): down_whole = jnp.concatenate(lax.all_gather(down_weight, 'sp'), axis=1)  15.1 us
    dot_general x1, matrix products, body(): jnp.dot(hidden, down_whole, preferred_element_type=jnp.float32)  14.6 us
    reduce_sum x4, other arithmetic, key_block(): totals = totals * shrink + jnp.sum(weights, axis=-1)  14.2 us
  transfers between devices with their start and end apart: 7, of which 7 were waited for; matrix products, arithmetic and copies ran while one was open for 4% of the time, Pallas kernels for 0%

profile of v1, /device:TPU:0, one launch (start us, length us, event | category | flops | bytes accessed | tf_op | source)
XLA Modules:
  0.0 663.3 jit_solution(6772892795275139343)
XLA Ops:
  10.4 1.3 pad_maximum_fusion.1
  15.1 67.4 %all-gather.7.cloned.1.call-done = bf16[3072,4,128]{2,1,0:T(4,128)(2,1)} async-done(((bf16[192,4,128]{2,1,0:T(4,128)(2,1)}), bf16[3072,4,128]{2,1,0:T(4,128)(2,1)}) %all-gather.7.cloned.1.call-update) | async-done | bytes 3145744 | tf_op jit(solution)/shard_map/all_gather | solution.py:91
  82.5 69.2 %all-gather.9.cloned.1.call-done = bf16[3072,4,128]{2,1,0:T(4,128)(2,1)} async-done(((bf16[192,4,128]{2,1,0:T(4,128)(2,1)}), bf16[3072,4,128]{2,1,0:T(4,128)(2,1)}) %all-gather.9.cloned.1.call-update) | async-done | bytes 3145744 | tf_op jit(solution)/shard_map/all_gather | solution.py:92
  151.7 40.1 %while.15 = (s32[]{:T(128)}, f32[4,2,192]{2,1,0:T(2,128)S(1)}, f32[4,2,192]{2,1,0:T(2,128)S(1)}, f32[4,2,192,128]{3,2,1,0:T(8,128)S(1)}, bf16[4,768,4,128]{3,2,1...) while((s32[]{:T(128)}, f32[4,2,192]{2,1,0:T(2,128)S(1)}, ...), condition=%wide.region_5.6_spmd.clone, body=%wide.region_2.5_spmd.clone.sunk | while | flops 614014464 | bytes 39813256 | solution.py:99
  151.7 1.9 constant_dynamic-slice_fusion.3
  153.6 2.9 bitcast_reduce_fusion.2
  156.5 3.5 fusion.42
  160.3 1.4 fusion.44
  161.7 1.9 constant_dynamic-slice_fusion.3
  163.6 2.9 bitcast_reduce_fusion.2
  166.6 3.5 fusion.42
  170.3 1.4 fusion.44
  171.7 1.9 constant_dynamic-slice_fusion.3
  173.6 2.9 bitcast_reduce_fusion.2
  176.6 3.5 fusion.42
  180.3 1.4 fusion.44
  181.7 1.9 constant_dynamic-slice_fusion.3
  183.7 2.9 bitcast_reduce_fusion.2
  186.6 3.5 fusion.42
  190.3 1.4 fusion.44
  192.8 4.1 convolution_convert_fusion.1
  198.7 5.1 reduce-scatter.3.cloned.1.call-done
  203.8 1.2 fusion.15
  205.2 2.5 all_gather.23
  207.7 141.2 %all-gather.15.cloned.1.call-done = bf16[45056,128]{1,0:T(8,128)(2,1)} async-done(((bf16[2816,128]{1,0:T(8,128)(2,1)}), bf16[45056,128]{1,0:T(8,128)(2,1)}) %all-gather.15.cloned.1.call-update) | async-done | bytes 11534352 | tf_op jit(solution)/shard_map/all_gather | solution.py:124
  348.9 15.1 %copy.60 = bf16[2816,16,128]{0,2,1:T(8,128)(2,1)} copy(bf16[2816,16,128]{2,0,1:T(8,128)(2,1)} %bitcast.62) | data formatting | bytes 23068672 | tf_op jit(solution)/shard_map/reshape | solution.py:124
  364.0 127.1 %all-gather.11.cloned.1.call-done = bf16[2048,2816]{1,0:T(8,128)(2,1)} async-done(((bf16[128,2816]{1,0:T(8,128)(2,1)}), bf16[2048,2816]{1,0:T(8,128)(2,1)}) %all-gather.11.cloned.1.call-update) | async-done | bytes 11534352 | tf_op jit(solution)/shard_map/all_gather | solution.py:121
  491.2 6.7 %fusion.24 = f32[192,2816]{1,0:T(8,128)S(1)} fusion(bf16[192,2048]{1,0:T(8,128)(2,1)S(1)} %all_gather.23, bf16[2048,2816]{1,0:T(8,128)(2,1)} %all-gather.11.cloned.1.call-done), kind=kOutput, calls=%fused_computation.69 | convolution fusion | flops 2214592512 | bytes 14483456 | tf_op jit(solution)/shard_map/dot_general | solution.py:119
  497.8 135.6 %all-gather.13.cloned.1.call-done = bf16[2048,2816]{1,0:T(8,128)(2,1)} async-done(((bf16[128,2816]{1,0:T(8,128)(2,1)}), bf16[2048,2816]{1,0:T(8,128)(2,1)}) %all-gather.13.cloned.1.call-update) | async-done | bytes 11534352 | tf_op jit(solution)/shard_map/all_gather | solution.py:122
  633.4 14.6 %convolution_convert_fusion = bf16[192,2048]{1,0:T(8,128)(2,1)} fusion(bf16[2816,2048]{0,1:T(8,128)(2,1)} %bitcast.63, bf16[192,2048]{1,0:T(8,128)(2,1)S(1)} %all_gather.23, bf16[2048,2816]{1,0:T(8,128)(2,1)} %all-gather.13.cloned.1.call-done, f32[192,2816]{1,0:T(8,128)S(1)} %fusion.24), kind=kOutput, calls=%fused_computation.23 | convolution fusion | flops 4432822272 | bytes 26804224 | tf_op jit(solution)/shard_map/dot_general | solution.py:126
  648.1 6.5 reduce-scatter.5.cloned.1.call-done
  654.6 1.9 fusion.18
  (74 shorter events, 10.8 us)
Async XLA Ops:
  6.5 5.2 copy-start.2
  6.5 6.1 copy-start.1
  6.5 75.9 %all-gather.7.cloned.1.call-start = ((), (), s32[]{:S(2)}) async-start(), calls=%async_computation.2 | async-start | bytes 3342336 | tf_op jit(solution)/shard_map/all_gather | solution.py:91
  8.0 5.3 copy-start.5
  11.7 140.0 %all-gather.9.cloned.1.call-start = ((), (), s32[]{:S(2)}) async-start(), calls=%async_computation.3 | async-start | bytes 3342336 | tf_op jit(solution)/shard_map/all_gather | solution.py:92
  12.5 191.2 %reduce-scatter.3.cloned.1.call-start = ((), (), s32[]{:S(2)}) async-start(), calls=%async_computation.4 | async-start | bytes 1179648 | tf_op jit(solution)/shard_map/reduce_scatter | solution.py:108
  156.5 3.8 copy-start
  166.5 3.8 copy-start
  176.6 3.8 copy-start
  186.6 3.8 copy-start
  192.5 11.3 %copy-start.3 = (bf16[192,2048]{1,0:T(8,128)(2,1)S(1)}, bf16[192,2048]{1,0:T(8,128)(2,1)}, u32[]{:S(2)}) copy-start(bf16[192,2048]{1,0:T(8,128)(2,1)} %param.13) | copy-start | bytes 2359300
  192.7 12.3 %copy-start.4 = (f32[2048]{0:T(1024)S(1)}, f32[2048]{0:T(1024)}, u32[]{:S(2)}) copy-start(f32[2048]{0:T(1024)} %param.20) | copy-start | bytes 24580
  196.9 152.0 %all-gather.15.cloned.1.call-start = ((), (), s32[]{:S(2)}) async-start(), calls=%async_computation.8 | async-start | bytes 12255232 | tf_op jit(solution)/shard_map/all_gather | solution.py:124
  197.5 293.7 %all-gather.11.cloned.1.call-start = ((), (), s32[]{:S(2)}) async-start(), calls=%async_computation.5 | async-start | bytes 12255232 | tf_op jit(solution)/shard_map/all_gather | solution.py:121
  198.1 435.4 %all-gather.13.cloned.1.call-start = ((), (), s32[]{:S(2)}) async-start(), calls=%async_computation.6 | async-start | bytes 12255232 | tf_op jit(solution)/shard_map/all_gather | solution.py:122
  198.6 455.9 %reduce-scatter.5.cloned.1.call-start = ((), (), s32[]{:S(2)}) async-start(), calls=%async_computation.7 | async-start | bytes 1179648 | tf_op jit(solution)/shard_map/reduce_scatter | solution.py:125
Sparse Core Ops, SparseCore 0:
  11.9 70.5 all-gather.6
  85.2 66.3 all-gather.8
  197.0 6.6 reduce-scatter.2
  206.4 142.5 all-gather.14
  351.5 139.5 all-gather.10
  493.8 139.5 all-gather.12
  648.2 6.3 reduce-scatter.4
